TPU v7x, 32 devices: a whole 2x2x4 slice. The times are simulated.
32 devices in a mesh: grp: 2 (over x), sp: 4 (over y, core), tp: 4 (over z).
Axes of the slice: x: 2, y: 2, z: 4, core: 2. Of those that a mesh axis runs over, the one named last changes fastest.
Arguments:
- layer_input: bfloat16 [8, 1024, 2048], P(('grp', 'tp'), 'sp'), parts along dimension 0, may hold values from -6 to 6
- norm_gain: bfloat16 [2048], replicated, may hold values from 0.099609375 to 1.8984375
- key_weight: bfloat16 [2048, 1024], replicated, may hold values from -0.125 to 0.125
- value_weight: bfloat16 [2048, 1024], replicated, may hold values from -0.125 to 0.125
- input_gate_weight: bfloat16 [2048, 8], replicated, may hold values from -0.125 to 0.125
- forget_gate_weight: bfloat16 [2048, 8], replicated, may hold values from -0.125 to 0.125
- conv_weight: float32 [4, 1024], replicated, may hold values from -3 to 3
- input_shift: float32 [8, 8, 1024], P(('grp', 'sp'), 'tp'), parts along dimension 0, may hold values from -4 to 302
- forget_shift: float32 [8, 8, 1024], P(('grp', 'sp'), 'tp'), parts along dimension 0, may hold values from 0 to 10.1
- new_query: bfloat16 [8, 8, 128], P(('grp', 'sp'), 'tp'), parts along dimension 0, may hold values from 0.1 to 2
- new_key: bfloat16 [8, 8, 128], P(('grp', 'sp'), 'tp'), parts along dimension 0, may hold values from -6 to 6
- new_value: bfloat16 [8, 8, 128], P(('grp', 'sp'), 'tp'), parts along dimension 0, may hold values from -6 to 6
- new_input: float32 [8, 8], P(('grp', 'sp'), 'tp'), parts along dimension 0, may hold values from 2 to 6
- new_forget: float32 [8, 8], P(('grp', 'sp'), 'tp'), parts along dimension 0, may hold values from -1 to 3
Outputs:
- key_cache: bfloat16 [8, 8, 1024, 128], P(('grp', 'sp'), 'tp'), parts along dimension 0
- value_cache: bfloat16 [8, 8, 1024, 128], P(('grp', 'sp'), 'tp'), parts along dimension 0
- weight_cache: float32 [8, 8, 1024], P(('grp', 'sp'), 'tp'), parts along dimension 0
- first_read: bfloat16 [8, 8, 128], P(('grp', 'sp'), 'tp'), parts along dimension 0
There are 2 independent parts, one for each index of `grp`. A program takes and returns all parts, laid end to end along the dimension named above; an argument that names none is the same for every part. Nothing has to cross between parts.
All inputs are finite; a program needn't handle non-finite values.
Results may differ from a plain program's by a relative error of at most 0.012.
Values may be sent and summed in bfloat16 or wider, within the bound.
A program may use at most 64 MiB of HBM per device.

v0:
```python
import jax
import jax.numpy as jnp
from jax import lax
from jax.sharding import PartitionSpec as P

HEADS = 8
DK = 128
CONV = 4
epsilon = 1e-06


def shifted(block, axis, distance):
    devices = range(lax.axis_size(axis))
    route = [(i - distance, i) for i in devices if i - distance in devices]
    return lax.ppermute(block, axis, route)


def project_rows(
    token_rows, norm_gain, key_weight, value_weight, input_gate_weight, forget_gate_weight
):
    widened = token_rows.astype(jnp.float32)
    normed = (
        widened
        * lax.rsqrt(jnp.mean(widened * widened, axis=-1, keepdims=True) + epsilon)
        * norm_gain.astype(jnp.float32)
    ).astype(jnp.bfloat16)
    key_matrix = key_weight.reshape(key_weight.shape[0], HEADS, DK)
    value_matrix = value_weight.reshape(value_weight.shape[0], HEADS, DK)
    key_linear = jnp.einsum(
        "apd,dhk->ahpk", normed, key_matrix, preferred_element_type=jnp.float32
    ).astype(jnp.bfloat16)
    values = jnp.einsum(
        "apd,dhk->ahpk", normed, value_matrix, preferred_element_type=jnp.float32
    ).astype(jnp.bfloat16)
    input_linear = jnp.einsum(
        "apd,dh->ahp", normed, input_gate_weight, preferred_element_type=jnp.float32
    ).astype(jnp.bfloat16)
    forget_linear = jnp.einsum(
        "apd,dh->ahp", normed, forget_gate_weight, preferred_element_type=jnp.float32
    ).astype(jnp.bfloat16)
    return (key_linear, values, input_linear, forget_linear)


def convolve(key_linear, previous, conv_weight):
    extended = jnp.concatenate([previous, key_linear], axis=2).astype(jnp.float32)
    length = key_linear.shape[2]
    tap_weight = conv_weight.reshape(CONV, HEADS, 1, DK)
    summed = extended[:, :, 0:length, :] * tap_weight[0]
    for offset in range(1, CONV):
        summed = summed + extended[:, :, offset : offset + length, :] * tap_weight[offset]
    return jax.nn.silu(summed).astype(jnp.bfloat16)


def read_cache(
    keys,
    values,
    input_linear,
    forget_linear,
    input_shift,
    forget_shift,
    new_query,
    new_key,
    new_value,
    new_input,
    new_forget,
):
    scaling = DK ** (-0.5)
    log_forget = jax.nn.log_sigmoid(forget_linear.astype(jnp.float32) + forget_shift)
    suffix = lax.cumsum(log_forget, axis=2, reverse=True) - log_forget
    new_decay = jax.nn.log_sigmoid(new_forget)
    log_weight = input_linear.astype(jnp.float32) + input_shift + suffix + new_decay[:, :, None]
    largest = jnp.maximum(jnp.max(log_weight, axis=2), new_input)
    weight_cache = jnp.exp(log_weight - largest[:, :, None])
    new_weight = jnp.exp(new_input - largest)
    matched = jnp.einsum("bhlk,bhk->bhl", keys, new_query, preferred_element_type=jnp.float32)
    scores = (weight_cache * matched * scaling).astype(jnp.bfloat16)
    fresh_match = jnp.sum(new_key.astype(jnp.float32) * new_query.astype(jnp.float32), axis=2)
    new_score = (new_weight * fresh_match * scaling).astype(jnp.bfloat16)
    denominator = jnp.sum(scores.astype(jnp.float32), axis=2) + new_score.astype(jnp.float32)
    numerator = jnp.einsum("bhl,bhlk->bhk", scores, values, preferred_element_type=jnp.float32)
    numerator = numerator + new_score.astype(jnp.float32)[:, :, None] * new_value.astype(
        jnp.float32
    )
    first_read = (numerator / jnp.maximum(jnp.abs(denominator), 1.0)[:, :, None]).astype(
        jnp.bfloat16
    )
    return (weight_cache, first_read)


def shards(
    layer_input,
    norm_gain,
    key_weight,
    value_weight,
    input_gate_weight,
    forget_gate_weight,
    conv_weight,
    input_shift,
    forget_shift,
    new_query,
    new_key,
    new_value,
    new_input,
    new_forget,
):
    key_linear, values, input_linear, forget_linear = project_rows(
        layer_input, norm_gain, key_weight, value_weight, input_gate_weight, forget_gate_weight
    )
    previous = shifted(key_linear[:, :, -(CONV - 1) :, :], "sp", 1)
    keys = convolve(key_linear, previous, conv_weight)
    keys, values, input_linear, forget_linear = (
        lax.all_to_all(
            lax.all_to_all(keys, "tp", split_axis=1, concat_axis=0, tiled=True),
            "sp",
            split_axis=0,
            concat_axis=2,
            tiled=True,
        ),
        lax.all_to_all(
            lax.all_to_all(values, "tp", split_axis=1, concat_axis=0, tiled=True),
            "sp",
            split_axis=0,
            concat_axis=2,
            tiled=True,
        ),
        lax.all_to_all(
            lax.all_to_all(input_linear, "tp", split_axis=1, concat_axis=0, tiled=True),
            "sp",
            split_axis=0,
            concat_axis=2,
            tiled=True,
        ),
        lax.all_to_all(
            lax.all_to_all(forget_linear, "tp", split_axis=1, concat_axis=0, tiled=True),
            "sp",
            split_axis=0,
            concat_axis=2,
            tiled=True,
        ),
    )
    weight_cache, first_read = read_cache(
        keys,
        values,
        input_linear,
        forget_linear,
        input_shift,
        forget_shift,
        new_query,
        new_key,
        new_value,
        new_input,
        new_forget,
    )
    return (keys, values, weight_cache, first_read)


def solution(mesh):
    in_specs = (
        P(("grp", "tp"), "sp", None),
        P(),
        P(),
        P(),
        P(),
        P(),
        P(),
        P(("grp", "sp"), "tp", None),
        P(("grp", "sp"), "tp", None),
        P(("grp", "sp"), "tp", None),
        P(("grp", "sp"), "tp", None),
        P(("grp", "sp"), "tp", None),
        P(("grp", "sp"), "tp"),
        P(("grp", "sp"), "tp"),
    )
    out_specs = (
        P(("grp", "sp"), "tp", None, None),
        P(("grp", "sp"), "tp", None, None),
        P(("grp", "sp"), "tp", None),
        P(("grp", "sp"), "tp", None),
    )
    return jax.shard_map(shards, mesh=mesh, in_specs=in_specs, out_specs=out_specs, check_vma=False)
```

profile of v0, /device:TPU:0, one launch (start us, length us, event | category | flops | bytes accessed | tf_op | source)
XLA Modules:
  0.0 106.6 jit_solution(14466072062410166473)
XLA Ops:
  0.6 0.0 copy-start
  0.6 0.0 copy-start.3
  0.7 0.0 copy-start.10
  0.7 0.8 convert_element_type.131
  1.4 1.5 %fusion.6 = f32[256]{0:T(256)S(1)} fusion(bf16[1,256,2048]{2,1,0:T(8,128)(2,1)} %param.14), kind=kLoop, calls=%fused_computation.8 | loop fusion | flops 1572608 | bytes 1049600 | tf_op jit(solution)/shard_map/reduce_sum | solution.py:24
  3.0 0.0 copy-done
  3.0 1.7 %fusion.22 = bf16[1,8,256]{2,1,0:T(8,128)(2,1)S(1)} fusion(bf16[2048,8]{0,1:T(8,128)(2,1)S(1)} %copy-done, bf16[1,256,2048]{2,1,0:T(8,128)(2,1)} %param.14, f32[2048]{0:T(1024)S(1)} %convert_element_type.131, f32[256]{0:T(256)S(1)} %add_rsqrt_fusion), kind=kOutput, calls=%fused_computation.18 | convolution fusion | flops 10487808 | bytes 1094656 | tf_op jit(solution)/shard_map/apd,dh->ahp/dot_general | solution.py:38
  4.7 0.5 broadcast.50
  5.2 0.7 reduce.10
  5.9 0.6 reshape.225
  6.5 6.3 %all-to-all-start.6 = ((bf16[4,2,256]{2,1,0:T(2,128)(2,1)}), bf16[4,2,256]{2,1,0:T(2,128)(2,1)S(1)}, u32[]{:S(2)}, u32[]{:S(2)}) async-start(bf16[4,2,256]{2,1,0:T(2,128)(2,1)} %reshape.225), calls=%async_computation.6 | async-start | bytes 8192 | tf_op jit(solution)/shard_map/all_to_all | solution.py:134
  12.8 0.0 copy-done.3
  12.8 0.0 copy-done.10
  12.8 0.4 fusion.21
  13.3 0.7 reduce.11
  14.0 0.6 reshape.227
  14.6 3.8 %all-to-all-done.6 = bf16[4,2,256]{2,1,0:T(2,128)(2,1)S(1)} async-done(((bf16[4,2,256]{2,1,0:T(2,128)(2,1)}), bf16[4,2,256]{2,1,0:T(2,128)(2,1)S(1)}, u32[]{:S(2)}, u32[]{:S(2)}) %all-to-all-start.6) | async-done | bytes 4128 | tf_op jit(solution)/shard_map/all_to_all | solution.py:134
  18.4 3.2 %all-to-all-start.4 = ((bf16[4,2,256]{2,1,0:T(2,128)(2,1)}), bf16[4,2,256]{2,1,0:T(2,128)(2,1)S(1)}, u32[]{:S(2)}, u32[]{:S(2)}) async-start(bf16[4,2,256]{2,1,0:T(2,128)(2,1)} %reshape.227), calls=%async_computation.4 | async-start | bytes 8192 | tf_op jit(solution)/shard_map/all_to_all | solution.py:127
  21.7 0.6 all_to_all.92
  22.3 4.9 %all-to-all-done.4 = bf16[4,2,256]{2,1,0:T(2,128)(2,1)S(1)} async-done(((bf16[4,2,256]{2,1,0:T(2,128)(2,1)}), bf16[4,2,256]{2,1,0:T(2,128)(2,1)S(1)}, u32[]{:S(2)}, u32[]{:S(2)}) %all-to-all-start.4) | async-done | bytes 4128 | tf_op jit(solution)/shard_map/all_to_all | solution.py:127
  27.2 3.2 %all-to-all-start.7 = ((bf16[4,2,256]{2,1,0:T(2,128)(2,1)}), bf16[4,2,256]{2,1,0:T(2,128)(2,1)S(1)}, u32[]{:S(2)}, u32[]{:S(2)}) async-start(bf16[4,2,256]{2,1,0:T(2,128)(2,1)} %all_to_all.92), calls=%async_computation.7 | async-start | bytes 8192 | tf_op jit(solution)/shard_map/all_to_all | solution.py:133
  30.5 0.6 all_to_all.89
  31.1 3.1 %all-to-all-done.7 = bf16[4,2,256]{2,1,0:T(2,128)(2,1)S(1)} async-done(((bf16[4,2,256]{2,1,0:T(2,128)(2,1)}), bf16[4,2,256]{2,1,0:T(2,128)(2,1)S(1)}, u32[]{:S(2)}, u32[]{:S(2)}) %all-to-all-start.7) | async-done | bytes 4128 | tf_op jit(solution)/shard_map/all_to_all | solution.py:133
  34.2 3.2 %all-to-all-start.5 = ((bf16[4,2,256]{2,1,0:T(2,128)(2,1)}), bf16[4,2,256]{2,1,0:T(2,128)(2,1)S(1)}, u32[]{:S(2)}, u32[]{:S(2)}) async-start(bf16[4,2,256]{2,1,0:T(2,128)(2,1)} %all_to_all.89), calls=%async_computation.5 | async-start | bytes 8192 | tf_op jit(solution)/shard_map/all_to_all | solution.py:126
  37.5 4.3 %fusion.15 = bf16[1,8,256,128]{3,2,0,1:T(8,128)(2,1)} fusion(bf16[1,256,2048]{2,1,0:T(8,128)(2,1)S(1)} %copy-done.3, f32[2048]{0:T(1024)S(1)} %convert_element_type.131, f32[256]{0:T(256)S(1)} %add_rsqrt_fusion, bf16[2048,1024]{1,0:T(8,128)(2,1)} %param.17), kind=kOutput, calls=%fused_computation.13 | convolution fusion | flops 1076101120 | bytes 5776384 | tf_op jit(solution)/shard_map/apd,dhk->ahpk/dot_general | solution.py:32
  41.8 0.0 all-to-all-done.5
  41.8 4.1 %all-to-all-start.2 = ((bf16[1,8,256,128]{3,2,0,1:T(8,128)(2,1)}), bf16[1,8,256,128]{3,2,0,1:T(8,128)(2,1)}, u32[]{:S(2)}, u32[]{:S(2)}) async-start(bf16[1,8,256,128]{3,2,0,1:T(8,128)(2,1)} %fusion.15), calls=%async_computation.2 | async-start | bytes 1048576 | tf_op jit(solution)/shard_map/all_to_all | solution.py:120
  45.9 0.0 copy-start.5
  45.9 3.5 %fusion.18 = bf16[1,8,256,128]{3,2,1,0:T(8,128)(2,1)S(1)} fusion(bf16[1,256,2048]{2,1,0:T(8,128)(2,1)S(1)} %copy-done.3, f32[2048]{0:T(1024)S(1)} %convert_element_type.131, f32[256]{0:T(256)S(1)} %add_rsqrt_fusion, bf16[2048,1024]{1,0:T(8,128)(2,1)} %param.16), kind=kOutput, calls=%fused_computation.14 | convolution fusion | flops 1076101120 | bytes 5776384 | tf_op jit(solution)/shard_map/apd,dhk->ahpk/dot_general | solution.py:29
  49.4 2.4 %collective-permute-start = (bf16[1,8,3,128]{3,2,1,0:T(4,128)(2,1)S(1)}, bf16[1,8,3,128]{3,2,1,0:T(4,128)(2,1)S(1)}, u32[]{:S(2)}, u32[]{:S(2)}) collective-permute-start(bf16[1,8,3,128]{3,2,1,0:T(4,128)(2,1)S(1)} %slice.48), channel_id=1, source_target_pairs={{0,4},{4,8},{8,12},{1,5},{5,9},{9,13},{2,6},{6,10},{10,14},{3,7},{... | collective-permute-start | bytes 18440 | tf_op jit(solution)/shard_map/ppermute | solution.py:15
  51.8 0.0 copy-done.5
  51.8 0.8 collective-permute-done
  52.6 0.1 maximum_convert_fusion
  52.7 0.0 copy-start.7
  52.7 0.0 copy-start.11
  52.8 0.0 copy-start.12
  52.8 0.0 copy-start.4
  52.8 1.5 %fusion.30 = bf16[1,8,256,128]{3,2,0,1:T(8,128)(2,1)} fusion(f32[8,128]{1,0:T(8,128)S(1)} %bitcast.172, f32[1,8,259,128]{3,2,1,0:T(8,128)S(1)} %maximum_convert_fusion, f32[8,128]{1,0:T(8,128)S(1)} %bitcast.173, f32[8,128]{1,0:T(8,128)S(1)} %bitcast.171, f32[8,128]{1,0:T(8,128)S(1)} %bitcast.170), kind=kLoop, calls=%fused_computation.32 | loop fusion | flops 3145728 | bytes 4734976 | tf_op jit(solution)/shard_map/convert_element_type | solution.py:51
  54.2 7.1 %all-to-all-done.2 = bf16[1,8,256,128]{3,2,0,1:T(8,128)(2,1)} async-done(((bf16[1,8,256,128]{3,2,0,1:T(8,128)(2,1)}), bf16[1,8,256,128]{3,2,0,1:T(8,128)(2,1)}, u32[]{:S(2)}, u32[]{:S(2)}) %all-to-all-start.2) | async-done | bytes 524320 | tf_op jit(solution)/shard_map/all_to_all | solution.py:120
  61.4 4.1 %all-to-all-start = ((bf16[1,8,256,128]{3,2,0,1:T(8,128)(2,1)}), bf16[1,8,256,128]{3,2,0,1:T(8,128)(2,1)}, u32[]{:S(2)}, u32[]{:S(2)}) async-start(bf16[1,8,256,128]{3,2,0,1:T(8,128)(2,1)} %fusion.30), calls=%async_computation | async-start | bytes 1048576 | tf_op jit(solution)/shard_map/all_to_all | solution.py:113
  65.5 0.0 copy-done.7
  65.5 0.0 copy-done.11
  65.5 0.1 multiply_reduce_fusion
  65.6 0.0 copy-done.12
  65.7 0.0 copy-done.4
  65.7 2.5 %reduce-window.6 = f32[1,2,8,128]{3,2,1,0:T(8,128)S(1)} reduce-window(f32[1,2,8,128]{3,2,1,0:T(8,128)S(1)} %copy.82, f32[]{:T(128)} %constant.7.clone.1), window={size=1x1x1x128 pad=0_0x0_0x0_0x0_127}, to_apply=%region_1.2 | reduce-window | flops 260096 | bytes 16388 | tf_op jit(solution)/shard_map/reduce-window
  68.2 0.1 slice_reduce_fusion
  68.3 0.2 reduce-window.9
  68.5 11.6 %all-to-all-done = bf16[1,8,256,128]{3,2,0,1:T(8,128)(2,1)} async-done(((bf16[1,8,256,128]{3,2,0,1:T(8,128)(2,1)}), bf16[1,8,256,128]{3,2,0,1:T(8,128)(2,1)}, u32[]{:S(2)}, u32[]{:S(2)}) %all-to-all-start) | async-done | bytes 524320 | tf_op jit(solution)/shard_map/all_to_all | solution.py:113
  80.1 3.5 %all-to-all-start.3 = ((bf16[4,2,256,128]{3,2,1,0:T(8,128)(2,1)}), bf16[4,2,256,128]{3,2,1,0:T(8,128)(2,1)S(1)}, u32[]{:S(2)}, u32[]{:S(2)}) async-start(bf16[4,2,256,128]{3,2,1,0:T(8,128)(2,1)} %bitcast.18), calls=%async_computation.3 | async-start | bytes 1048576 | tf_op jit(solution)/shard_map/all_to_all | solution.py:119
  83.6 0.1 slice_bitcast_fusion
  83.6 0.1 broadcast.41
  83.7 8.6 %all-to-all-done.3 = bf16[4,2,256,128]{3,2,1,0:T(8,128)(2,1)S(1)} async-done(((bf16[4,2,256,128]{3,2,1,0:T(8,128)(2,1)}), bf16[4,2,256,128]{3,2,1,0:T(8,128)(2,1)S(1)}, u32[]{:S(2)}, u32[]{:S(2)}) %all-to-all-start.3) | async-done | bytes 524320 | tf_op jit(solution)/shard_map/all_to_all | solution.py:119
  92.3 3.6 %all-to-all-start.1 = ((bf16[4,2,256,128]{3,2,1,0:T(8,128)(2,1)}), bf16[4,2,256,128]{3,2,1,0:T(8,128)(2,1)S(1)}, u32[]{:S(2)}, u32[]{:S(2)}) async-start(bf16[4,2,256,128]{3,2,1,0:T(8,128)(2,1)} %bitcast.10), calls=%async_computation.1 | async-start | bytes 1048576 | tf_op jit(solution)/shard_map/all_to_all | solution.py:112
  96.0 0.0 copy-done.6
  96.0 0.2 fusion.55
  96.2 0.0 copy-done.8
  96.2 0.0 copy-start.1
  96.2 8.5 %all-to-all-done.1 = bf16[4,2,256,128]{3,2,1,0:T(8,128)(2,1)S(1)} async-done(((bf16[4,2,256,128]{3,2,1,0:T(8,128)(2,1)}), bf16[4,2,256,128]{3,2,1,0:T(8,128)(2,1)S(1)}, u32[]{:S(2)}, u32[]{:S(2)}) %all-to-all-start.1) | async-done | bytes 524320 | tf_op jit(solution)/shard_map/all_to_all | solution.py:112
  104.8 0.0 copy-start.2
  104.8 0.2 fusion.36
  105.0 0.8 convert_reduce_fusion
  105.8 0.2 fusion.34
  106.0 0.6 fusion.38
  (26 shorter events, 0.3 us)
Async XLA Ops:
  0.6 2.3 %copy-start = (bf16[2048,8]{0,1:T(8,128)(2,1)S(1)}, bf16[2048,8]{0,1:T(8,128)(2,1)}, u32[]{:S(2)}) copy-start(bf16[2048,8]{0,1:T(8,128)(2,1)} %param.19) | copy-start | bytes 98308
  0.6 12.2 %copy-start.3 = (bf16[1,256,2048]{2,1,0:T(8,128)(2,1)S(1)}, bf16[1,256,2048]{2,1,0:T(8,128)(2,1)}, u32[]{:S(2)}) copy-start(bf16[1,256,2048]{2,1,0:T(8,128)(2,1)} %param.14) | copy-start | bytes 3145732
  0.7 12.2 %copy-start.10 = (bf16[2048,8]{0,1:T(8,128)(2,1)S(1)}, bf16[2048,8]{0,1:T(8,128)(2,1)}, u32[]{:S(2)}) copy-start(bf16[2048,8]{0,1:T(8,128)(2,1)} %param.18) | copy-start | bytes 98308
  6.5 11.9 %all-to-all-start.6 = ((bf16[4,2,256]{2,1,0:T(2,128)(2,1)}), bf16[4,2,256]{2,1,0:T(2,128)(2,1)S(1)}, u32[]{:S(2)}, u32[]{:S(2)}) async-start(bf16[4,2,256]{2,1,0:T(2,128)(2,1)} %reshape.225), calls=%async_computation.6 | async-start | bytes 8192 | tf_op jit(solution)/shard_map/all_to_all | solution.py:134
  18.4 8.8 %all-to-all-start.4 = ((bf16[4,2,256]{2,1,0:T(2,128)(2,1)}), bf16[4,2,256]{2,1,0:T(2,128)(2,1)S(1)}, u32[]{:S(2)}, u32[]{:S(2)}) async-start(bf16[4,2,256]{2,1,0:T(2,128)(2,1)} %reshape.227), calls=%async_computation.4 | async-start | bytes 8192 | tf_op jit(solution)/shard_map/all_to_all | solution.py:127
  27.2 7.0 %all-to-all-start.7 = ((bf16[4,2,256]{2,1,0:T(2,128)(2,1)}), bf16[4,2,256]{2,1,0:T(2,128)(2,1)S(1)}, u32[]{:S(2)}, u32[]{:S(2)}) async-start(bf16[4,2,256]{2,1,0:T(2,128)(2,1)} %all_to_all.92), calls=%async_computation.7 | async-start | bytes 8192 | tf_op jit(solution)/shard_map/all_to_all | solution.py:133
  34.2 7.5 %all-to-all-start.5 = ((bf16[4,2,256]{2,1,0:T(2,128)(2,1)}), bf16[4,2,256]{2,1,0:T(2,128)(2,1)S(1)}, u32[]{:S(2)}, u32[]{:S(2)}) async-start(bf16[4,2,256]{2,1,0:T(2,128)(2,1)} %all_to_all.89), calls=%async_computation.5 | async-start | bytes 8192 | tf_op jit(solution)/shard_map/all_to_all | solution.py:126
  41.8 19.6 %all-to-all-start.2 = ((bf16[1,8,256,128]{3,2,0,1:T(8,128)(2,1)}), bf16[1,8,256,128]{3,2,0,1:T(8,128)(2,1)}, u32[]{:S(2)}, u32[]{:S(2)}) async-start(bf16[1,8,256,128]{3,2,0,1:T(8,128)(2,1)} %fusion.15), calls=%async_computation.2 | async-start | bytes 1048576 | tf_op jit(solution)/shard_map/all_to_all | solution.py:120
  45.9 5.9 %copy-start.5 = (f32[4,1024]{1,0:T(4,128)S(1)}, f32[4,1024]{1,0:T(4,128)}, u32[]{:S(2)}) copy-start(f32[4,1024]{1,0:T(4,128)} %param.20) | copy-start | bytes 49156
  49.4 3.2 %collective-permute-start = (bf16[1,8,3,128]{3,2,1,0:T(4,128)(2,1)S(1)}, bf16[1,8,3,128]{3,2,1,0:T(4,128)(2,1)S(1)}, u32[]{:S(2)}, u32[]{:S(2)}) collective-permute-start(bf16[1,8,3,128]{3,2,1,0:T(4,128)(2,1)S(1)} %slice.48), channel_id=1, source_target_pairs={{0,4},{4,8},{8,12},{1,5},{5,9},{9,13},{2,6},{6,10},{10,14},{3,7},{... | collective-permute-start | bytes 18440 | tf_op jit(solution)/shard_map/ppermute | solution.py:15
  52.7 12.8 %copy-start.7 = (bf16[1,2,128]{2,1,0:T(2,128)(2,1)S(1)}, bf16[1,2,128]{2,1,0:T(2,128)(2,1)}, u32[]{:S(2)}) copy-start(bf16[1,2,128]{2,1,0:T(2,128)(2,1)} %param.23) | copy-start | bytes 1540
  52.7 12.8 %copy-start.11 = (bf16[1,2,128]{2,1,0:T(2,128)(2,1)S(1)}, bf16[1,2,128]{2,1,0:T(2,128)(2,1)}, u32[]{:S(2)}) copy-start(bf16[1,2,128]{2,1,0:T(2,128)(2,1)} %param.24) | copy-start | bytes 1540
  52.8 12.9 %copy-start.12 = (f32[1,2]{1,0:T(1,128)S(1)}, f32[1,2]{1,0:T(1,128)}, u32[]{:S(2)}) copy-start(f32[1,2]{1,0:T(1,128)} %param.27) | copy-start | bytes 28
  52.8 12.9 %copy-start.4 = (f32[1,2,1024]{2,1,0:T(2,128)S(1)}, f32[1,2,1024]{2,1,0:T(2,128)}, u32[]{:S(2)}) copy-start(f32[1,2,1024]{2,1,0:T(2,128)} %param.22) | copy-start | bytes 24580
  54.2 41.7 %copy-start.6 = (f32[1,2,1024]{2,1,0:T(2,128)S(1)}, f32[1,2,1024]{2,1,0:T(2,128)}, u32[]{:S(2)}) copy-start(f32[1,2,1024]{2,1,0:T(2,128)} %param.21) | copy-start | bytes 24580
  54.2 41.9 %copy-start.8 = (f32[1,2]{1,0:T(1,128)S(1)}, f32[1,2]{1,0:T(1,128)}, u32[]{:S(2)}) copy-start(f32[1,2]{1,0:T(1,128)} %param.26) | copy-start | bytes 28
  61.4 18.7 %all-to-all-start = ((bf16[1,8,256,128]{3,2,0,1:T(8,128)(2,1)}), bf16[1,8,256,128]{3,2,0,1:T(8,128)(2,1)}, u32[]{:S(2)}, u32[]{:S(2)}) async-start(bf16[1,8,256,128]{3,2,0,1:T(8,128)(2,1)} %fusion.30), calls=%async_computation | async-start | bytes 1048576 | tf_op jit(solution)/shard_map/all_to_all | solution.py:113
  80.1 12.3 %all-to-all-start.3 = ((bf16[4,2,256,128]{3,2,1,0:T(8,128)(2,1)}), bf16[4,2,256,128]{3,2,1,0:T(8,128)(2,1)S(1)}, u32[]{:S(2)}, u32[]{:S(2)}) async-start(bf16[4,2,256,128]{3,2,1,0:T(8,128)(2,1)} %bitcast.18), calls=%async_computation.3 | async-start | bytes 1048576 | tf_op jit(solution)/shard_map/all_to_all | solution.py:119
  92.3 13.7 %copy-start.9 = (bf16[1,2,128]{2,1,0:T(2,128)(2,1)S(1)}, bf16[1,2,128]{2,1,0:T(2,128)(2,1)}, u32[]{:S(2)}) copy-start(bf16[1,2,128]{2,1,0:T(2,128)(2,1)} %param.25) | copy-start | bytes 1540
  92.3 12.4 %all-to-all-start.1 = ((bf16[4,2,256,128]{3,2,1,0:T(8,128)(2,1)}), bf16[4,2,256,128]{3,2,1,0:T(8,128)(2,1)S(1)}, u32[]{:S(2)}, u32[]{:S(2)}) async-start(bf16[4,2,256,128]{3,2,1,0:T(8,128)(2,1)} %bitcast.10), calls=%async_computation.1 | async-start | bytes 1048576 | tf_op jit(solution)/shard_map/all_to_all | solution.py:112
  96.2 10.4 %copy-start.1 = (bf16[4,2,256,128]{3,2,0,1:T(8,128)(2,1)}, bf16[4,2,256,128]{3,2,0,1:T(8,128)(2,1)S(1)}, u32[]{:S(2)}) copy-start(bf16[4,2,256,128]{3,2,0,1:T(8,128)(2,1)S(1)} %copy.45) | copy-start | bytes 1572868
  104.8 1.9 %copy-start.2 = (bf16[4,2,256,128]{3,2,0,1:T(8,128)(2,1)}, bf16[4,2,256,128]{3,2,0,1:T(8,128)(2,1)S(1)}, u32[]{:S(2)}) copy-start(bf16[4,2,256,128]{3,2,0,1:T(8,128)(2,1)S(1)} %copy.42) | copy-start | bytes 1572868
where the time goes:
time: 107 us
  waiting for transfers between devices  48.4 us (45%)
  starting transfers between devices  33.8 us (32%)
  matrix products  10.3 us (10%)
  other arithmetic  9.68 us (9%)
  local copies, waits for them, and re-layouts  3.49 us (3%)
    all_to_all x1, waiting for transfers between devices, shards(): lax.all_to_all(keys, 'tp', split_axis=1, concat_axis=0, tiled=True)  11.6 us
    all_to_all x1, waiting for transfers between devices, shards(): lax.all_to_all(lax.all_to_all(values, 'tp', split_axis=1, concat_axis=0,...  8.61 us
    all_to_all x1, waiting for transfers between devices, shards(): lax.all_to_all(lax.all_to_all(keys, 'tp', split_axis=1, concat_axis=0, ti...  8.51 us
    all_to_all x1, waiting for transfers between devices, shards(): lax.all_to_all(values, 'tp', split_axis=1, concat_axis=0, tiled=True)  7.12 us
    all_to_all x1, starting transfers between devices, shards(): lax.all_to_all(forget_linear, 'tp', split_axis=1, concat_axis=0, tiled=True)  6.35 us
    all_to_all x1, waiting for transfers between devices, shards(): lax.all_to_all(input_linear, 'tp', split_axis=1, concat_axis=0, tiled=True)  4.89 us
    dot_general x1, matrix products, project_rows(): jnp.einsum('apd,dhk->ahpk', normed, value_matrix, preferred_element_type=...  4.29 us
    all_to_all x1, starting transfers between devices, shards(): lax.all_to_all(values, 'tp', split_axis=1, concat_axis=0, tiled=True)  4.14 us
  transfers between devices with their start and end apart: 9, of which 8 were waited for; matrix products, arithmetic and copies ran while one was open for 14% of the time, Pallas kernels for 0%

commit v1 on v0

--- a/solution.py
+++ b/solution.py
@@ -2,11 +2,23 @@
 import jax.numpy as jnp
 from jax import lax
 from jax.sharding import PartitionSpec as P
+from jax.lax import axis_index, axis_size, ppermute
 
 HEADS = 8
 DK = 128
 CONV = 4
 epsilon = 1e-06
+
+
+def solve_points(sample, dim_at, body):
+    fresh, mixed_arr = (sample.shape[:dim_at], sample.shape[dim_at + 1 :])
+    return jnp.moveaxis(sample.reshape(*fresh, body, -1, *mixed_arr), dim_at, 0)
+
+
+def map_task(w_in, dim_k):
+    finding = list(w_in.shape[1:])
+    finding[dim_k] *= w_in.shape[0]
+    return jnp.moveaxis(w_in, 0, dim_k).reshape(finding)
 
 
 def shifted(block, axis, distance):
@@ -103,6 +115,21 @@
     new_input,
     new_forget,
 ):
+
+    def update_tails(a0, group_axis, view, vector):
+        o_now, spare = (axis_size(group_axis), axis_index(group_axis))
+        right_arr = solve_points(a0, view, o_now)
+        all_rows = [right_arr[spare]]
+        for to_i in range(1, o_now):
+            far_arr = right_arr[(spare + to_i) % o_now]
+            all_rows.append(
+                ppermute(
+                    far_arr, group_axis, [(dev_i, (dev_i + to_i) % o_now) for dev_i in range(o_now)]
+                )
+            )
+        right_arr = jnp.stack(all_rows)[(spare - jnp.arange(o_now)) % o_now]
+        return map_task(right_arr, vector)
+
     key_linear, values, input_linear, forget_linear = project_rows(
         layer_input, norm_gain, key_weight, value_weight, input_gate_weight, forget_gate_weight
     )
@@ -131,11 +158,7 @@
             tiled=True,
         ),
         lax.all_to_all(
-            lax.all_to_all(forget_linear, "tp", split_axis=1, concat_axis=0, tiled=True),
-            "sp",
-            split_axis=0,
-            concat_axis=2,
-            tiled=True,
+            update_tails(forget_linear, "tp", 1, 0), "sp", split_axis=0, concat_axis=2, tiled=True
         ),
     )
     weight_cache, first_read = read_cache(

time: 107 us -> 103 us (0.963)
  waiting for transfers between devices: 48.4 us -> 44 us
    all_to_all x2 -> x1, starting transfers between devices: 9.59 us -> 3.25 us  [shards(): lax.all_to_all(update_tails(forget_linear, 'tp', 1, 0), 'sp', split_axis=...]
    ppermute x0 -> x3, starting transfers between devices: none -> 6.14 us  [update_tails(): ppermute(far_arr, group_axis, [(dev_i, (dev_i + to_i) % o_now) for dev_i...]
    all_to_all x2 -> x1, waiting for transfers between devices: 6.92 us -> 3.1 us  [shards(): lax.all_to_all(update_tails(forget_linear, 'tp', 1, 0), 'sp', split_axis=...]
    gather x0 -> x1, local copies, waits for them, and re-layouts: none -> 1.16 us  [update_tails(): right_arr = jnp.stack(all_rows)[(spare - jnp.arange(o_now)) % o_now]]
    another operation x2 -> x3, other arithmetic: 2.68 us -> 2.7 us
  transfers between devices with their start and end apart: 9 -> 11, of which waited for: 8 -> 7; matrix products, arithmetic and copies ran while one was open for 14% -> 16% of each run, Pallas kernels for 0% -> 0%
where the time goes in v1:
time: 103 us; the launch traced here: 102 us
  waiting for transfers between devices  44 us (43%)
  starting transfers between devices  34.4 us (33%)
  matrix products  10.3 us (10%)
  other arithmetic  9.03 us (9%)
  local copies, waits for them, and re-layouts  3.4 us (3%)
  between operations  1.03 us (1%)
    all_to_all x1, waiting for transfers between devices, shards(): lax.all_to_all(keys, 'tp', split_axis=1, concat_axis=0, tiled=True)  11.6 us
    all_to_all x1, waiting for transfers between devices, shards(): lax.all_to_all(lax.all_to_all(values, 'tp', split_axis=1, concat_axis=0,...  8.61 us
    all_to_all x1, waiting for transfers between devices, shards(): lax.all_to_all(lax.all_to_all(keys, 'tp', split_axis=1, concat_axis=0, ti...  8.51 us
    all_to_all x1, waiting for transfers between devices, shards(): lax.all_to_all(values, 'tp', split_axis=1, concat_axis=0, tiled=True)  7.11 us
    ppermute x3, starting transfers between devices, update_tails(): ppermute(far_arr, group_axis, [(dev_i, (dev_i + to_i) % o_now) for dev_i...  6.14 us
    all_to_all x1, waiting for transfers between devices, shards(): lax.all_to_all(input_linear, 'tp', split_axis=1, concat_axis=0, tiled=True)  4.34 us
    dot_general x1, matrix products, project_rows(): jnp.einsum('apd,dhk->ahpk', normed, value_matrix, preferred_element_type=...  4.29 us
    all_to_all x1, starting transfers between devices, shards(): lax.all_to_all(keys, 'tp', split_axis=1, concat_axis=0, tiled=True)  4.14 us
  transfers between devices with their start and end apart: 11, of which 7 were waited for; matrix products, arithmetic and copies ran while one was open for 16% of the time, Pallas kernels for 0%

profile of v1, /device:TPU:0, one launch (start us, length us, event | category | flops | bytes accessed | tf_op | source)
XLA Modules:
  0.0 102.2 jit_solution(8638553539271028213)
XLA Ops:
  0.6 0.0 copy-start
  0.6 0.0 copy-start.3
  0.7 0.0 copy-start.10
  0.7 0.8 convert_element_type.129
  1.5 1.5 %fusion.6 = f32[256]{0:T(256)S(1)} fusion(bf16[1,256,2048]{2,1,0:T(8,128)(2,1)} %param.14), kind=kLoop, calls=%fused_computation.9 | loop fusion | flops 1572608 | bytes 1049600 | tf_op jit(solution)/shard_map/reduce_sum | solution.py:36
  3.0 0.0 copy-done
  3.0 1.7 %fusion.22 = bf16[8,256]{1,0:T(8,128)(2,1)S(1)} fusion(bf16[2048,8]{0,1:T(8,128)(2,1)S(1)} %copy-done, bf16[1,256,2048]{2,1,0:T(8,128)(2,1)} %param.14, f32[2048]{0:T(1024)S(1)} %convert_element_type.129, f32[256]{0:T(256)S(1)} %add_rsqrt_fusion), kind=kOutput, calls=%fused_computation.19 | convolution fusion | flops 10487808 | bytes 1094656 | tf_op jit(solution)/shard_map/apd,dh->ahp/dot_general | solution.py:50
  4.7 5.1 %collective-permute-start.3 = (bf16[1,2,256]{2,1,0:T(2,128)(2,1)S(1)}, bf16[1,2,256]{2,1,0:T(2,128)(2,1)S(1)}, u32[]{:S(2)}, u32[]{:S(2)}) collective-permute-start(bf16[1,2,256]{2,1,0:T(2,128)(2,1)S(1)} %get-tuple-element.16), channel_id=1, source_target_pairs={{0,3},{1,0},{2,1},{3,2},{4,7},{5,4},{6,5},{7,6},{8,11},{9,8},{10,9... | collective-permute-start | bytes 3080 | tf_op jit(solution)/shard_map/ppermute | solution.py:126
  9.8 0.0 collective-permute-start.2
  9.8 1.0 collective-permute-start.1
  10.9 0.0 copy-done.3
  10.9 0.0 copy-done.10
  10.9 0.4 fusion.21
  11.3 0.5 broadcast.121
  11.8 0.7 reduce.8
  12.5 0.6 reshape.286
  13.1 4.1 %all-to-all-start.4 = ((bf16[4,2,256]{2,1,0:T(2,128)(2,1)}), bf16[4,2,256]{2,1,0:T(2,128)(2,1)S(1)}, u32[]{:S(2)}, u32[]{:S(2)}) async-start(bf16[4,2,256]{2,1,0:T(2,128)(2,1)} %reshape.286), calls=%async_computation.4 | async-start | bytes 8192 | tf_op jit(solution)/shard_map/all_to_all | solution.py:154
  17.2 0.0 collective-permute-done.3
  17.2 0.0 collective-permute-done.2
  17.3 0.0 collective-permute-done.1
  17.3 1.2 %gather_fusion = bf16[4,2,256]{2,1,0:T(2,128)(2,1)} fusion(bf16[4,2,256]{2,1,0:T(2,128)(2,1)S(1)} %maximum_bitcast_fusion, s32[1024]{0:T(1024)S(1)} %pad_clamp_fusion), kind=kCustom, calls=%fused_computation | custom fusion | bytes 8208 | tf_op jit(solution)/shard_map/gather | solution.py:130
  18.5 4.3 %all-to-all-done.4 = bf16[4,2,256]{2,1,0:T(2,128)(2,1)S(1)} async-done(((bf16[4,2,256]{2,1,0:T(2,128)(2,1)}), bf16[4,2,256]{2,1,0:T(2,128)(2,1)S(1)}, u32[]{:S(2)}, u32[]{:S(2)}) %all-to-all-start.4) | async-done | bytes 4128 | tf_op jit(solution)/shard_map/all_to_all | solution.py:154
  22.8 3.2 %all-to-all-start.6 = ((bf16[4,2,256]{2,1,0:T(2,128)(2,1)}), bf16[4,2,256]{2,1,0:T(2,128)(2,1)S(1)}, u32[]{:S(2)}, u32[]{:S(2)}) async-start(bf16[4,2,256]{2,1,0:T(2,128)(2,1)} %gather_fusion), calls=%async_computation.6 | async-start | bytes 8192 | tf_op jit(solution)/shard_map/all_to_all | solution.py:160
  26.1 0.6 all_to_all.80
  26.7 3.1 %all-to-all-done.6 = bf16[4,2,256]{2,1,0:T(2,128)(2,1)S(1)} async-done(((bf16[4,2,256]{2,1,0:T(2,128)(2,1)}), bf16[4,2,256]{2,1,0:T(2,128)(2,1)S(1)}, u32[]{:S(2)}, u32[]{:S(2)}) %all-to-all-start.6) | async-done | bytes 4128 | tf_op jit(solution)/shard_map/all_to_all | solution.py:160
  29.8 3.2 %all-to-all-start.5 = ((bf16[4,2,256]{2,1,0:T(2,128)(2,1)}), bf16[4,2,256]{2,1,0:T(2,128)(2,1)S(1)}, u32[]{:S(2)}, u32[]{:S(2)}) async-start(bf16[4,2,256]{2,1,0:T(2,128)(2,1)} %all_to_all.80), calls=%async_computation.5 | async-start | bytes 8192 | tf_op jit(solution)/shard_map/all_to_all | solution.py:153
  33.1 4.3 %fusion.15 = bf16[1,8,256,128]{3,2,0,1:T(8,128)(2,1)} fusion(bf16[1,256,2048]{2,1,0:T(8,128)(2,1)S(1)} %copy-done.3, f32[2048]{0:T(1024)S(1)} %convert_element_type.129, f32[256]{0:T(256)S(1)} %add_rsqrt_fusion, bf16[2048,1024]{1,0:T(8,128)(2,1)} %param.17), kind=kOutput, calls=%fused_computation.14 | convolution fusion | flops 1076101120 | bytes 5776384 | tf_op jit(solution)/shard_map/apd,dhk->ahpk/dot_general | solution.py:44
  37.4 0.0 all-to-all-done.5
  37.4 4.1 %all-to-all-start.2 = ((bf16[1,8,256,128]{3,2,0,1:T(8,128)(2,1)}), bf16[1,8,256,128]{3,2,0,1:T(8,128)(2,1)}, u32[]{:S(2)}, u32[]{:S(2)}) async-start(bf16[1,8,256,128]{3,2,0,1:T(8,128)(2,1)} %fusion.15), calls=%async_computation.2 | async-start | bytes 1048576 | tf_op jit(solution)/shard_map/all_to_all | solution.py:147
  41.5 0.0 copy-start.5
  41.5 3.5 %fusion.18 = bf16[1,8,256,128]{3,2,1,0:T(8,128)(2,1)S(1)} fusion(bf16[1,256,2048]{2,1,0:T(8,128)(2,1)S(1)} %copy-done.3, f32[2048]{0:T(1024)S(1)} %convert_element_type.129, f32[256]{0:T(256)S(1)} %add_rsqrt_fusion, bf16[2048,1024]{1,0:T(8,128)(2,1)} %param.16), kind=kOutput, calls=%fused_computation.15 | convolution fusion | flops 1076101120 | bytes 5776384 | tf_op jit(solution)/shard_map/apd,dhk->ahpk/dot_general | solution.py:41
  45.0 2.3 %collective-permute-start = (bf16[1,8,3,128]{3,2,1,0:T(4,128)(2,1)S(1)}, bf16[1,8,3,128]{3,2,1,0:T(4,128)(2,1)S(1)}, u32[]{:S(2)}, u32[]{:S(2)}) collective-permute-start(bf16[1,8,3,128]{3,2,1,0:T(4,128)(2,1)S(1)} %slice.50), channel_id=1, source_target_pairs={{0,4},{4,8},{8,12},{1,5},{5,9},{9,13},{2,6},{6,10},{10,14},{3,7},{... | collective-permute-start | bytes 18440 | tf_op jit(solution)/shard_map/ppermute | solution.py:27
  47.4 0.0 copy-done.5
  47.4 0.8 collective-permute-done
  48.2 0.1 maximum_convert_fusion
  48.3 0.0 copy-start.7
  48.3 0.0 copy-start.11
  48.3 0.0 copy-start.12
  48.4 0.0 copy-start.4
  48.4 1.5 %fusion.30 = bf16[1,8,256,128]{3,2,0,1:T(8,128)(2,1)} fusion(f32[8,128]{1,0:T(8,128)S(1)} %bitcast.177, f32[1,8,259,128]{3,2,1,0:T(8,128)S(1)} %maximum_convert_fusion, f32[8,128]{1,0:T(8,128)S(1)} %bitcast.178, f32[8,128]{1,0:T(8,128)S(1)} %bitcast.176, f32[8,128]{1,0:T(8,128)S(1)} %bitcast.175), kind=kLoop, calls=%fused_computation.33 | loop fusion | flops 3145728 | bytes 4734976 | tf_op jit(solution)/shard_map/convert_element_type | solution.py:63
  49.8 7.1 %all-to-all-done.2 = bf16[1,8,256,128]{3,2,0,1:T(8,128)(2,1)} async-done(((bf16[1,8,256,128]{3,2,0,1:T(8,128)(2,1)}), bf16[1,8,256,128]{3,2,0,1:T(8,128)(2,1)}, u32[]{:S(2)}, u32[]{:S(2)}) %all-to-all-start.2) | async-done | bytes 524320 | tf_op jit(solution)/shard_map/all_to_all | solution.py:147
  56.9 4.1 %all-to-all-start = ((bf16[1,8,256,128]{3,2,0,1:T(8,128)(2,1)}), bf16[1,8,256,128]{3,2,0,1:T(8,128)(2,1)}, u32[]{:S(2)}, u32[]{:S(2)}) async-start(bf16[1,8,256,128]{3,2,0,1:T(8,128)(2,1)} %fusion.30), calls=%async_computation | async-start | bytes 1048576 | tf_op jit(solution)/shard_map/all_to_all | solution.py:140
  61.1 0.0 copy-done.7
  61.1 0.0 copy-done.11
  61.1 0.1 multiply_reduce_fusion
  61.2 0.0 copy-done.12
  61.3 0.0 copy-done.4
  61.3 2.5 %reduce-window.6 = f32[1,2,8,128]{3,2,1,0:T(8,128)S(1)} reduce-window(f32[1,2,8,128]{3,2,1,0:T(8,128)S(1)} %copy.79, f32[]{:T(128)} %constant.53.clone.1), window={size=1x1x1x128 pad=0_0x0_0x0_0x0_127}, to_apply=%region_1.2 | reduce-window | flops 260096 | bytes 16388 | tf_op jit(solution)/shard_map/reduce-window
  63.8 0.1 slice_reduce_fusion
  63.9 0.2 reduce-window.9
  64.1 11.6 %all-to-all-done = bf16[1,8,256,128]{3,2,0,1:T(8,128)(2,1)} async-done(((bf16[1,8,256,128]{3,2,0,1:T(8,128)(2,1)}), bf16[1,8,256,128]{3,2,0,1:T(8,128)(2,1)}, u32[]{:S(2)}, u32[]{:S(2)}) %all-to-all-start) | async-done | bytes 524320 | tf_op jit(solution)/shard_map/all_to_all | solution.py:140
  75.7 3.5 %all-to-all-start.3 = ((bf16[4,2,256,128]{3,2,1,0:T(8,128)(2,1)}), bf16[4,2,256,128]{3,2,1,0:T(8,128)(2,1)S(1)}, u32[]{:S(2)}, u32[]{:S(2)}) async-start(bf16[4,2,256,128]{3,2,1,0:T(8,128)(2,1)} %bitcast.18), calls=%async_computation.3 | async-start | bytes 1048576 | tf_op jit(solution)/shard_map/all_to_all | solution.py:146
  79.2 0.1 slice_bitcast_fusion
  79.2 0.1 broadcast.108
  79.3 8.6 %all-to-all-done.3 = bf16[4,2,256,128]{3,2,1,0:T(8,128)(2,1)S(1)} async-done(((bf16[4,2,256,128]{3,2,1,0:T(8,128)(2,1)}), bf16[4,2,256,128]{3,2,1,0:T(8,128)(2,1)S(1)}, u32[]{:S(2)}, u32[]{:S(2)}) %all-to-all-start.3) | async-done | bytes 524320 | tf_op jit(solution)/shard_map/all_to_all | solution.py:146
  87.9 3.6 %all-to-all-start.1 = ((bf16[4,2,256,128]{3,2,1,0:T(8,128)(2,1)}), bf16[4,2,256,128]{3,2,1,0:T(8,128)(2,1)S(1)}, u32[]{:S(2)}, u32[]{:S(2)}) async-start(bf16[4,2,256,128]{3,2,1,0:T(8,128)(2,1)} %bitcast.10), calls=%async_computation.1 | async-start | bytes 1048576 | tf_op jit(solution)/shard_map/all_to_all | solution.py:139
  91.6 0.2 fusion.57
  91.8 0.0 copy-start.1
  91.8 8.5 %all-to-all-done.1 = bf16[4,2,256,128]{3,2,1,0:T(8,128)(2,1)S(1)} async-done(((bf16[4,2,256,128]{3,2,1,0:T(8,128)(2,1)}), bf16[4,2,256,128]{3,2,1,0:T(8,128)(2,1)S(1)}, u32[]{:S(2)}, u32[]{:S(2)}) %all-to-all-start.1) | async-done | bytes 524320 | tf_op jit(solution)/shard_map/all_to_all | solution.py:139
  100.4 0.0 copy-start.2
  100.4 0.2 fusion.36
  100.6 0.8 convert_reduce_fusion
  101.4 0.2 fusion.34
  101.6 0.6 fusion.38
  (30 shorter events, 0.3 us)
Async XLA Ops:
  0.6 2.4 %copy-start = (bf16[2048,8]{0,1:T(8,128)(2,1)S(1)}, bf16[2048,8]{0,1:T(8,128)(2,1)}, u32[]{:S(2)}) copy-start(bf16[2048,8]{0,1:T(8,128)(2,1)} %param.19) | copy-start | bytes 98308
  0.6 10.2 %copy-start.3 = (bf16[1,256,2048]{2,1,0:T(8,128)(2,1)S(1)}, bf16[1,256,2048]{2,1,0:T(8,128)(2,1)}, u32[]{:S(2)}) copy-start(bf16[1,256,2048]{2,1,0:T(8,128)(2,1)} %param.14) | copy-start | bytes 3145732
  0.7 10.2 %copy-start.10 = (bf16[2048,8]{0,1:T(8,128)(2,1)S(1)}, bf16[2048,8]{0,1:T(8,128)(2,1)}, u32[]{:S(2)}) copy-start(bf16[2048,8]{0,1:T(8,128)(2,1)} %param.18) | copy-start | bytes 98308
  4.7 12.5 %collective-permute-start.3 = (bf16[1,2,256]{2,1,0:T(2,128)(2,1)S(1)}, bf16[1,2,256]{2,1,0:T(2,128)(2,1)S(1)}, u32[]{:S(2)}, u32[]{:S(2)}) collective-permute-start(bf16[1,2,256]{2,1,0:T(2,128)(2,1)S(1)} %get-tuple-element.16), channel_id=1, source_target_pairs={{0,3},{1,0},{2,1},{3,2},{4,7},{5,4},{6,5},{7,6},{8,11},{9,8},{10,9... | collective-permute-start | bytes 3080 | tf_op jit(solution)/shard_map/ppermute | solution.py:126
  9.8 7.4 %collective-permute-start.2 = (bf16[1,2,256]{2,1,0:T(2,128)(2,1)S(1)}, bf16[1,2,256]{2,1,0:T(2,128)(2,1)S(1)}, u32[]{:S(2)}, u32[]{:S(2)}) collective-permute-start(bf16[1,2,256]{2,1,0:T(2,128)(2,1)S(1)} %get-tuple-element.17), channel_id=1, source_target_pairs={{0,2},{1,3},{2,0},{3,1},{4,6},{5,7},{6,4},{7,5},{8,10},{9,11},{10,... | collective-permute-start | bytes 3080 | tf_op jit(solution)/shard_map/ppermute | solution.py:126
  9.8 7.4 %collective-permute-start.1 = (bf16[1,2,256]{2,1,0:T(2,128)(2,1)S(1)}, bf16[1,2,256]{2,1,0:T(2,128)(2,1)S(1)}, u32[]{:S(2)}, u32[]{:S(2)}) collective-permute-start(bf16[1,2,256]{2,1,0:T(2,128)(2,1)S(1)} %get-tuple-element.18), channel_id=1, source_target_pairs={{0,1},{1,2},{2,3},{3,0},{4,5},{5,6},{6,7},{7,4},{8,9},{9,10},{10,1... | collective-permute-start | bytes 3080 | tf_op jit(solution)/shard_map/ppermute | solution.py:126
  13.1 9.7 %all-to-all-start.4 = ((bf16[4,2,256]{2,1,0:T(2,128)(2,1)}), bf16[4,2,256]{2,1,0:T(2,128)(2,1)S(1)}, u32[]{:S(2)}, u32[]{:S(2)}) async-start(bf16[4,2,256]{2,1,0:T(2,128)(2,1)} %reshape.286), calls=%async_computation.4 | async-start | bytes 8192 | tf_op jit(solution)/shard_map/all_to_all | solution.py:154
  22.8 7.0 %all-to-all-start.6 = ((bf16[4,2,256]{2,1,0:T(2,128)(2,1)}), bf16[4,2,256]{2,1,0:T(2,128)(2,1)S(1)}, u32[]{:S(2)}, u32[]{:S(2)}) async-start(bf16[4,2,256]{2,1,0:T(2,128)(2,1)} %gather_fusion), calls=%async_computation.6 | async-start | bytes 8192 | tf_op jit(solution)/shard_map/all_to_all | solution.py:160
  29.8 7.6 %all-to-all-start.5 = ((bf16[4,2,256]{2,1,0:T(2,128)(2,1)}), bf16[4,2,256]{2,1,0:T(2,128)(2,1)S(1)}, u32[]{:S(2)}, u32[]{:S(2)}) async-start(bf16[4,2,256]{2,1,0:T(2,128)(2,1)} %all_to_all.80), calls=%async_computation.5 | async-start | bytes 8192 | tf_op jit(solution)/shard_map/all_to_all | solution.py:153
  37.4 19.6 %all-to-all-start.2 = ((bf16[1,8,256,128]{3,2,0,1:T(8,128)(2,1)}), bf16[1,8,256,128]{3,2,0,1:T(8,128)(2,1)}, u32[]{:S(2)}, u32[]{:S(2)}) async-start(bf16[1,8,256,128]{3,2,0,1:T(8,128)(2,1)} %fusion.15), calls=%async_computation.2 | async-start | bytes 1048576 | tf_op jit(solution)/shard_map/all_to_all | solution.py:147
  41.5 5.9 %copy-start.5 = (f32[4,1024]{1,0:T(4,128)S(1)}, f32[4,1024]{1,0:T(4,128)}, u32[]{:S(2)}) copy-start(f32[4,1024]{1,0:T(4,128)} %param.20) | copy-start | bytes 49156
  45.0 3.2 %collective-permute-start = (bf16[1,8,3,128]{3,2,1,0:T(4,128)(2,1)S(1)}, bf16[1,8,3,128]{3,2,1,0:T(4,128)(2,1)S(1)}, u32[]{:S(2)}, u32[]{:S(2)}) collective-permute-start(bf16[1,8,3,128]{3,2,1,0:T(4,128)(2,1)S(1)} %slice.50), channel_id=1, source_target_pairs={{0,4},{4,8},{8,12},{1,5},{5,9},{9,13},{2,6},{6,10},{10,14},{3,7},{... | collective-permute-start | bytes 18440 | tf_op jit(solution)/shard_map/ppermute | solution.py:27
  48.3 12.8 %copy-start.7 = (bf16[1,2,128]{2,1,0:T(2,128)(2,1)S(1)}, bf16[1,2,128]{2,1,0:T(2,128)(2,1)}, u32[]{:S(2)}) copy-start(bf16[1,2,128]{2,1,0:T(2,128)(2,1)} %param.23) | copy-start | bytes 1540
  48.3 12.8 %copy-start.11 = (bf16[1,2,128]{2,1,0:T(2,128)(2,1)S(1)}, bf16[1,2,128]{2,1,0:T(2,128)(2,1)}, u32[]{:S(2)}) copy-start(bf16[1,2,128]{2,1,0:T(2,128)(2,1)} %param.24) | copy-start | bytes 1540
  48.3 12.9 %copy-start.12 = (f32[1,2]{1,0:T(1,128)S(1)}, f32[1,2]{1,0:T(1,128)}, u32[]{:S(2)}) copy-start(f32[1,2]{1,0:T(1,128)} %param.27) | copy-start | bytes 28
  48.4 12.9 %copy-start.4 = (f32[1,2,1024]{2,1,0:T(2,128)S(1)}, f32[1,2,1024]{2,1,0:T(2,128)}, u32[]{:S(2)}) copy-start(f32[1,2,1024]{2,1,0:T(2,128)} %param.22) | copy-start | bytes 24580
  49.8 41.7 %copy-start.6 = (f32[1,2,1024]{2,1,0:T(2,128)S(1)}, f32[1,2,1024]{2,1,0:T(2,128)}, u32[]{:S(2)}) copy-start(f32[1,2,1024]{2,1,0:T(2,128)} %param.21) | copy-start | bytes 24580
  49.8 41.9 %copy-start.8 = (f32[1,2]{1,0:T(1,128)S(1)}, f32[1,2]{1,0:T(1,128)}, u32[]{:S(2)}) copy-start(f32[1,2]{1,0:T(1,128)} %param.26) | copy-start | bytes 28
  56.9 18.7 %all-to-all-start = ((bf16[1,8,256,128]{3,2,0,1:T(8,128)(2,1)}), bf16[1,8,256,128]{3,2,0,1:T(8,128)(2,1)}, u32[]{:S(2)}, u32[]{:S(2)}) async-start(bf16[1,8,256,128]{3,2,0,1:T(8,128)(2,1)} %fusion.30), calls=%async_computation | async-start | bytes 1048576 | tf_op jit(solution)/shard_map/all_to_all | solution.py:140
  75.7 12.3 %all-to-all-start.3 = ((bf16[4,2,256,128]{3,2,1,0:T(8,128)(2,1)}), bf16[4,2,256,128]{3,2,1,0:T(8,128)(2,1)S(1)}, u32[]{:S(2)}, u32[]{:S(2)}) async-start(bf16[4,2,256,128]{3,2,1,0:T(8,128)(2,1)} %bitcast.18), calls=%async_computation.3 | async-start | bytes 1048576 | tf_op jit(solution)/shard_map/all_to_all | solution.py:146
  87.9 13.7 %copy-start.9 = (bf16[1,2,128]{2,1,0:T(2,128)(2,1)S(1)}, bf16[1,2,128]{2,1,0:T(2,128)(2,1)}, u32[]{:S(2)}) copy-start(bf16[1,2,128]{2,1,0:T(2,128)(2,1)} %param.25) | copy-start | bytes 1540
  87.9 12.4 %all-to-all-start.1 = ((bf16[4,2,256,128]{3,2,1,0:T(8,128)(2,1)}), bf16[4,2,256,128]{3,2,1,0:T(8,128)(2,1)S(1)}, u32[]{:S(2)}, u32[]{:S(2)}) async-start(bf16[4,2,256,128]{3,2,1,0:T(8,128)(2,1)} %bitcast.10), calls=%async_computation.1 | async-start | bytes 1048576 | tf_op jit(solution)/shard_map/all_to_all | solution.py:139
  91.8 10.4 %copy-start.1 = (bf16[4,2,256,128]{3,2,0,1:T(8,128)(2,1)}, bf16[4,2,256,128]{3,2,0,1:T(8,128)(2,1)S(1)}, u32[]{:S(2)}) copy-start(bf16[4,2,256,128]{3,2,0,1:T(8,128)(2,1)S(1)} %copy.44) | copy-start | bytes 1572868
  100.4 1.9 %copy-start.2 = (bf16[4,2,256,128]{3,2,0,1:T(8,128)(2,1)}, bf16[4,2,256,128]{3,2,0,1:T(8,128)(2,1)S(1)}, u32[]{:S(2)}) copy-start(bf16[4,2,256,128]{3,2,0,1:T(8,128)(2,1)S(1)} %copy.41) | copy-start | bytes 1572868
